TPU v7x, 32 devices: a whole 2x2x4 slice. The times are simulated.
32 devices in a mesh: sp: 8 (over z, x), tp: 4 (over y, core).
Axes of the slice: x: 2, y: 2, z: 4, core: 2. Of those that a mesh axis runs over, the one named last changes fastest.
Arguments:
- queries: bfloat16 [5120, 2048], P('sp', 'tp'), may hold values from -164 to 164
- keys: bfloat16 [5120, 512], P('sp', 'tp'), may hold values from -6 to 6
- values: bfloat16 [5120, 512], P('sp', 'tp'), may hold values from -6 to 6
- sink: float32 [32], P('tp'), may hold values from 4 to 8
- stream: bfloat16 [5120, 2048], P(('sp', 'tp')), may hold values from -6 to 6
- out_weight: bfloat16 [2048, 2048], P('tp'), may hold values from -0.5390625 to 0.5390625
- norm_gain: float32 [2048], replicated, may hold values from 0.1 to 1.9
- gate_weight: bfloat16 [2048, 5632], P('sp', 'tp'), may hold values from -0.125 to 0.125
- up_weight: bfloat16 [2048, 5632], P('sp', 'tp'), may hold values from -0.125 to 0.125
- down_weight: bfloat16 [5632, 2048], P('tp', 'sp'), may hold values from -0.23925781 to 0.23925781
Outputs:
- result: bfloat16 [5120, 2048], P(('sp', 'tp'))
All inputs are finite; a program needn't handle non-finite values.
Results may differ from a plain program's by a relative error of at most 0.019.
Values may be sent and summed in bfloat16 or wider, within the bound.
A program may use at most 128 MiB of HBM per device.

v0:
```python
import jax
import jax.numpy as jnp
from jax import lax
from jax.sharding import PartitionSpec as P

HEAD = 64
WINDOW = 128


def padded_2(cells, sides, width):
    for axis, dim in sides:
        count = lax.axis_size(axis)
        ends = count - 1
        head = lax.slice_in_dim(cells, 0, width, axis=dim)
        tail = lax.slice_in_dim(cells, cells.shape[dim] - width, cells.shape[dim], axis=dim)
        cells = jnp.concatenate(
            [
                lax.ppermute(tail, axis, [(i, (i + 1) % count) for i in range(ends)]),
                cells,
                lax.ppermute(head, axis, [((i + 1) % count, i) for i in range(ends)]),
            ],
            axis=dim,
        )
    return cells


def rotary(block, start):
    length = block.shape[0]
    middle = HEAD // 2
    inverse = 1.0 / 10000.0 ** (jnp.arange(0, HEAD, 2, dtype=jnp.float32) / HEAD)
    places = (start + jnp.arange(length, dtype=jnp.int32)).astype(jnp.float32)
    angles = places[:, None, None] * inverse[None, None, :]
    cosine_table = jnp.cos(angles)
    sine_table = jnp.sin(angles)
    pieces = block.astype(jnp.float32).reshape(length, -1, HEAD)
    leading = pieces[..., :middle]
    trailing = pieces[..., middle:]
    turned = jnp.concatenate(
        [
            leading * cosine_table - trailing * sine_table,
            trailing * cosine_table + leading * sine_table,
        ],
        -1,
    )
    return turned.reshape(length, -1).astype(jnp.bfloat16)


def window_attend(queries, keys, values, sink):
    rows_here = queries.shape[0]
    start = lax.axis_index("sp") * rows_here
    length = lax.axis_size("sp") * rows_here
    blocks = rows_here // WINDOW
    kv_width = keys.shape[1]
    kv_count = kv_width // HEAD
    head_count = queries.shape[1] // HEAD
    group = head_count // kv_count
    turned_q = rotary(queries, start)
    turned_k = rotary(keys, start)
    paired = jnp.concatenate([turned_k, values], 1)
    padded = padded_2(paired, (("sp", 0),), WINDOW)
    framed = padded.reshape(blocks + 2, WINDOW, 2 * kv_width)
    banded = jnp.concatenate([framed[:-2], framed[1:-1], framed[2:]], axis=1)
    key_band = banded[..., :kv_width].reshape(blocks, 3 * WINDOW, kv_count, HEAD)
    value_band = banded[..., kv_width:].reshape(blocks, 3 * WINDOW, kv_count, HEAD)
    query_blocks = turned_q.reshape(blocks, WINDOW, kv_count, group, HEAD)
    scores = jnp.einsum(
        "nqkgd,nskd->nkgqs", query_blocks, key_band, preferred_element_type=jnp.float32
    ) * HEAD ** (-0.5)
    query_place = (
        start + jnp.arange(blocks)[:, None, None] * WINDOW + jnp.arange(WINDOW)[None, :, None]
    )
    key_place = (
        start
        + jnp.arange(blocks)[:, None, None] * WINDOW
        - WINDOW
        + jnp.arange(3 * WINDOW)[None, None, :]
    )
    valid = (jnp.abs(key_place - query_place) <= WINDOW) & (key_place >= 0) & (key_place < length)
    scores = jnp.where(valid[:, None, None], scores, -jnp.inf)
    sink_grid = sink.reshape(kv_count, group)[None, :, :, None]
    top = jnp.maximum(jnp.max(scores, -1), sink_grid)
    raised = jnp.exp(scores - top[..., None])
    denom = jnp.sum(raised, -1) + jnp.exp(sink_grid - top)
    weights = (raised / denom[..., None]).astype(jnp.bfloat16)
    output = jnp.einsum(
        "nkgqs,nskd->nqkgd", weights, value_band, preferred_element_type=jnp.float32
    )
    return output.astype(jnp.bfloat16).reshape(rows_here, head_count * HEAD)


def collect_weights(gate_weight, up_weight, down_weight):
    return (
        lax.all_gather(gate_weight, "sp", axis=0, tiled=True),
        lax.all_gather(up_weight, "sp", axis=0, tiled=True),
        lax.all_gather(down_weight, "sp", axis=1, tiled=True),
    )


def local(
    queries, keys, values, sink, stream, out_weight, norm_gain, gate_weight, up_weight, down_weight
):
    attended = window_attend(queries, keys, values, sink)
    gathered = collect_weights(gate_weight, up_weight, down_weight)
    gate_whole, up_whole, down_whole = gathered
    rows = attended
    projected = lax.psum_scatter(
        jnp.dot(rows, out_weight, preferred_element_type=jnp.float32),
        "tp",
        scatter_dimension=0,
        tiled=True,
    )
    mixed = (stream.astype(jnp.float32) + projected).astype(jnp.bfloat16)
    mixed_wide = mixed.astype(jnp.float32)
    scale = lax.rsqrt(jnp.mean(mixed_wide * mixed_wide, -1, keepdims=True) + 1e-06)
    normed = (mixed_wide * scale * norm_gain).astype(jnp.bfloat16)
    piece = lax.all_gather(normed, "tp", axis=0, tiled=True)
    gate = jnp.dot(piece, gate_whole, preferred_element_type=jnp.float32)
    upward = jnp.dot(piece, up_whole, preferred_element_type=jnp.float32)
    hidden = (jax.nn.silu(gate) * upward).astype(jnp.bfloat16)
    rows = hidden
    lowered = lax.psum_scatter(
        jnp.dot(rows, down_whole, preferred_element_type=jnp.float32).astype(jnp.bfloat16),
        "tp",
        scatter_dimension=0,
        tiled=True,
    ).astype(jnp.float32)
    return (mixed_wide + 0.5 * lowered).astype(jnp.bfloat16)


def solution(mesh):
    placed = (
        P("sp", "tp"),
        P("sp", "tp"),
        P("sp", "tp"),
        P("tp"),
        P(("sp", "tp"), None),
        P("tp", None),
        P(),
        P("sp", "tp"),
        P("sp", "tp"),
        P("tp", "sp"),
    )
    return jax.shard_map(
        local, mesh=mesh, in_specs=placed, out_specs=P(("sp", "tp"), None), check_vma=False
    )
```

profile of v0, /device:TPU:0, one launch (start us, length us, event | category | flops | bytes accessed | tf_op | source)
XLA Modules:
  0.0 420.8 jit_solution(13338107045309871906)
XLA Ops:
  7.4 1.2 copy.24
  8.6 1.1 copy.25
  9.7 0.4 multiply_cosine_fusion
  10.2 0.7 fusion.17
  10.9 5.5 %collective-permute-start = (bf16[128,256]{0,1:T(8,128)(2,1)}, bf16[128,256]{0,1:T(8,128)(2,1)}, u32[]{:S(2)}, u32[]{:S(2)}) collective-permute-start(bf16[128,256]{0,1:T(8,128)(2,1)} %get-tuple-element.16), channel_id=1, source_target_pairs={{0,4},{4,8},{8,12},{12,16},{16,20},{20,24},{24,28},{1,5},{5,9},{9,... | collective-permute-start | bytes 196616 | tf_op jit(solution)/shard_map/ppermute | solution.py:18
  16.4 1.3 collective-permute-start.1
  17.7 0.1 fusion.20
  17.7 0.1 iota_add_fusion
  17.8 0.1 iota_add_fusion.1
  17.9 1.4 copy.31
  19.3 0.1 convert.19
  19.4 0.2 subtract_convert_fusion
  19.5 1.2 fusion.11
  20.7 0.9 pad_maximum_fusion.1
  21.6 1.8 convert_element_type.55
  23.4 1.3 max.17
  24.8 2.1 pad_maximum_fusion.5
  26.8 1.9 copy.26
  28.7 1.9 copy.27
  30.6 1.9 copy.28
  32.5 1.2 pad_maximum_fusion
  33.7 1.2 fusion.24
  34.9 2.0 copy.30
  36.9 2.3 fusion.1
  39.2 0.1 broadcast_maximum_fusion
  39.3 1.9 fusion
  41.2 1.1 copy-done.1
  42.3 0.1 exponential_add_fusion
  42.4 0.3 copy.29
  42.6 5.4 %fusion.9 = bf16[5,128,2,4,64]{1,4,3,2,0:T(8,128)(2,1)S(1)} fusion(bf16[5,384,2,64,1]{1,3,4,2,0:T(8,128)(2,1)S(1)} %bitcast.59, f32[5,2,384,128,4]{3,2,4,1,0:T(8,128)} %copy-done.1, f32[5,2,4,128]{3,2,1,0:T(4,128)S(1)} %exponential_add_fusion, f32[5,2,4,128]{3,2,1,0:T(4,128)S(1)} %broadcast_maximum_fusion, pred[5,128,384]{1,2,0:T(8,128)(4,1)S(1)} %fusion.11), kind=kOutput, calls=%fused_computation.18 | convolution fusion | flops 261816320 | bytes 9297920 | tf_op jit(solution)/shard_map/nkgqs,nskd->nqkgd/dot_general | solution.py:85
  48.1 0.5 copy.34
  48.5 4.0 fusion.12
  52.5 0.0 all-gather.7.cloned.1.call-start
  52.6 0.5 all-gather.7.cloned.1.call-update
  53.2 53.3 %reduce-scatter.3.cloned.1.call-done = f32[160,2048]{1,0:T(8,128)} async-done(((f32[640,2048]{1,0:T(8,128)}), f32[160,2048]{1,0:T(8,128)}) %reduce-scatter.3.cloned.1.call-update) | async-done | bytes 1310736 | tf_op jit(solution)/shard_map/reduce_scatter | solution.py:106
  106.4 1.6 fusion.5
  108.0 1.1 fusion.7
  109.2 0.5 all-gather.11.cloned.1.call-update
  109.8 0.7 all-gather.9.cloned.1.call-update
  110.4 0.2 reduce-scatter.5.cloned.1.call-start
  110.7 39.1 %all-gather.7.cloned.1.call-done = bf16[2048,1408]{1,0:T(8,128)(2,1)} async-done(((bf16[256,1408]{1,0:T(8,128)(2,1)}), bf16[2048,1408]{1,0:T(8,128)(2,1)}) %all-gather.7.cloned.1.call-update) | async-done | bytes 5767184 | tf_op jit(solution)/shard_map/all_gather | solution.py:93
  149.8 25.0 %all-gather.5.cloned.1.call-done = bf16[640,2048]{1,0:T(8,128)(2,1)} async-done(((bf16[160,2048]{1,0:T(8,128)(2,1)}), bf16[640,2048]{1,0:T(8,128)(2,1)}) %all-gather.5.cloned.1.call-update) | async-done | bytes 2621456 | tf_op jit(solution)/shard_map/all_gather | solution.py:116
  174.8 9.4 %fusion.25 = f32[640,1408]{1,0:T(8,128)} fusion(bf16[640,2048]{1,0:T(8,128)(2,1)} %all-gather.5.cloned.1.call-done, bf16[2048,1408]{1,0:T(8,128)(2,1)} %all-gather.7.cloned.1.call-done), kind=kOutput, calls=%fused_computation.62 | convolution fusion | flops 3690987520 | bytes 11993088 | tf_op jit(solution)/shard_map/dot_general | solution.py:117
  184.2 85.4 %all-gather.11.cloned.1.call-done = bf16[1408,2048]{1,0:T(8,128)(2,1)} async-done(((bf16[1408,256]{1,0:T(8,128)(2,1)}), bf16[1408,2048]{1,0:T(8,128)(2,1)}) %all-gather.11.cloned.1.call-update) | async-done | bytes 5767184 | tf_op jit(solution)/shard_map/all_gather | solution.py:95
  269.6 92.5 %all-gather.9.cloned.1.call-done = bf16[2048,1408]{1,0:T(8,128)(2,1)} async-done(((bf16[256,1408]{1,0:T(8,128)(2,1)}), bf16[2048,1408]{1,0:T(8,128)(2,1)}) %all-gather.9.cloned.1.call-update) | async-done | bytes 5767184 | tf_op jit(solution)/shard_map/all_gather | solution.py:94
  362.1 16.1 %convolution_convert_fusion = bf16[640,2048]{1,0:T(8,128)(2,1)} fusion(bf16[1408,2048]{1,0:T(8,128)(2,1)} %all-gather.11.cloned.1.call-done, bf16[640,2048]{1,0:T(8,128)(2,1)} %all-gather.5.cloned.1.call-done, bf16[2048,1408]{1,0:T(8,128)(2,1)} %all-gather.9.cloned.1.call-done, f32[640,1408]{1,0:T(8,128)} %fusion.25), kind=kOutput, calls=%fused_computation.8 | convolution fusion | flops 7388692480 | bytes 20381696 | tf_op jit(solution)/shard_map/dot_general | solution.py:122
  378.3 32.8 %reduce-scatter.5.cloned.1.call-done = bf16[160,2048]{1,0:T(8,128)(2,1)} async-done(((bf16[640,2048]{1,0:T(8,128)(2,1)}), bf16[160,2048]{1,0:T(8,128)(2,1)}) %reduce-scatter.5.cloned.1.call-update) | async-done | bytes 655376 | tf_op jit(solution)/shard_map/reduce_scatter | solution.py:121
  411.1 2.1 fusion.8
  (29 shorter events, 0.3 us)
Async XLA Ops:
  7.4 41.2 %copy-start = (bf16[512,2048]{1,0:T(8,128)(2,1)S(1)}, bf16[512,2048]{1,0:T(8,128)(2,1)}, u32[]{:S(2)}) copy-start(bf16[512,2048]{1,0:T(8,128)(2,1)} %param.15) | copy-start | bytes 6291460
  7.4 99.1 %reduce-scatter.3.cloned.1.call-start = ((), (), s32[]{:S(2)}) async-start(), calls=%async_computation.2 | async-start | bytes 6553600 | tf_op jit(solution)/shard_map/reduce_scatter | solution.py:106
  10.2 7.6 %copy-start.3 = (bf16[640,2,64]{0,2,1:T(8,128)(2,1)}, bf16[640,2,64]{0,2,1:T(8,128)(2,1)S(1)}, u32[]{:S(2)}) copy-start(bf16[640,2,64]{0,2,1:T(8,128)(2,1)S(1)} %pad_maximum_fusion.7) | copy-start | bytes 491524
  10.9 13.9 %collective-permute-start = (bf16[128,256]{0,1:T(8,128)(2,1)}, bf16[128,256]{0,1:T(8,128)(2,1)}, u32[]{:S(2)}, u32[]{:S(2)}) collective-permute-start(bf16[128,256]{0,1:T(8,128)(2,1)} %get-tuple-element.16), channel_id=1, source_target_pairs={{0,4},{4,8},{8,12},{12,16},{16,20},{20,24},{24,28},{1,5},{5,9},{9,... | collective-permute-start | bytes 196616 | tf_op jit(solution)/shard_map/ppermute | solution.py:18
  16.4 8.4 %collective-permute-start.1 = (bf16[128,256]{0,1:T(8,128)(2,1)}, bf16[128,256]{0,1:T(8,128)(2,1)}, u32[]{:S(2)}, u32[]{:S(2)}) collective-permute-start(bf16[128,256]{0,1:T(8,128)(2,1)} %get-tuple-element.17), channel_id=1, source_target_pairs={{4,0},{8,4},{12,8},{16,12},{20,16},{24,20},{28,24},{5,1},{9,5},{13... | collective-permute-start | bytes 196616 | tf_op jit(solution)/shard_map/ppermute | solution.py:20
  36.9 2.3 copy-start.6
  39.2 3.1 copy-start.1
  39.3 3.0 copy-start.2
  52.5 53.9 %copy-start.4 = (bf16[160,2048]{1,0:T(8,128)(2,1)S(1)}, bf16[160,2048]{1,0:T(8,128)(2,1)}, u32[]{:S(2)}) copy-start(bf16[160,2048]{1,0:T(8,128)(2,1)} %param.14) | copy-start | bytes 1966084
  52.5 55.5 %copy-start.5 = (f32[2048]{0:T(1024)S(1)}, f32[2048]{0:T(1024)}, u32[]{:S(2)}) copy-start(f32[2048]{0:T(1024)} %param.16) | copy-start | bytes 24580
  52.5 97.2 %all-gather.7.cloned.1.call-start = ((), (), s32[]{:S(2)}) async-start(), calls=%async_computation.4 | async-start | bytes 6488064 | tf_op jit(solution)/shard_map/all_gather | solution.py:93
  53.1 121.7 %all-gather.5.cloned.1.call-start = ((), (), s32[]{:S(2)}) async-start(), calls=%async_computation.3 | async-start | bytes 3276800 | tf_op jit(solution)/shard_map/all_gather | solution.py:116
  109.1 160.5 %all-gather.11.cloned.1.call-start = ((), (), s32[]{:S(2)}) async-start(), calls=%async_computation.6 | async-start | bytes 6488064 | tf_op jit(solution)/shard_map/all_gather | solution.py:95
  109.7 252.4 %all-gather.9.cloned.1.call-start = ((), (), s32[]{:S(2)}) async-start(), calls=%async_computation.5 | async-start | bytes 6488064 | tf_op jit(solution)/shard_map/all_gather | solution.py:94
  110.4 300.6 %reduce-scatter.5.cloned.1.call-start = ((), (), s32[]{:S(2)}) async-start(), calls=%async_computation.7 | async-start | bytes 3276800 | tf_op jit(solution)/shard_map/reduce_scatter | solution.py:121
Sparse Core Ops, SparseCore 0:
  52.7 53.7 reduce-scatter.2
  378.4 32.6 reduce-scatter.4
Sparse Core Ops, SparseCore 1:
  55.2 94.5 all-gather.6
  151.2 23.5 all-gather.4
  176.7 92.8 all-gather.10
  271.8 90.3 all-gather.8
where the time goes:
time: 421 us
  waiting for transfers between devices  330 us (78%)
  matrix products  37.2 us (9%)
  local copies, waits for them, and re-layouts  17.4 us (4%)
  between operations  15.2 us (4%)
  other arithmetic  13.9 us (3%)
  starting transfers between devices  7.16 us (2%)
    all_gather x1, waiting for transfers between devices, collect_weights(): lax.all_gather(up_weight, 'sp', axis=0, tiled=True)  92.5 us
    all_gather x1, waiting for transfers between devices, collect_weights(): lax.all_gather(down_weight, 'sp', axis=1, tiled=True)  85.4 us
    reduce_scatter x1, waiting for transfers between devices, local(): lax.psum_scatter(jnp.dot(rows, out_weight, preferred_element_type=jnp.flo...  53.3 us
    all_gather x1, waiting for transfers between devices, collect_weights(): lax.all_gather(gate_weight, 'sp', axis=0, tiled=True)  39.1 us
    reduce_scatter x1, waiting for transfers between devices, local(): lax.psum_scatter(jnp.dot(rows, down_whole, preferred_element_type=jnp.flo...  32.8 us
    all_gather x1, waiting for transfers between devices, local(): piece = lax.all_gather(normed, 'tp', axis=0, tiled=True)  25 us
    dot_general x1, matrix products, local(): jnp.dot(rows, down_whole, preferred_element_type=jnp.float32)  16.1 us
    dot_general x1, matrix products, local(): gate = jnp.dot(piece, gate_whole, preferred_element_type=jnp.float32)  9.43 us
  transfers between devices with their start and end apart: 8, of which 6 were waited for; matrix products, arithmetic and copies ran while one was open for 5% of the time, Pallas kernels for 0%

commit v1 on v0

--- a/solution.py
+++ b/solution.py
@@ -113,7 +113,12 @@
     mixed_wide = mixed.astype(jnp.float32)
     scale = lax.rsqrt(jnp.mean(mixed_wide * mixed_wide, -1, keepdims=True) + 1e-06)
     normed = (mixed_wide * scale * norm_gain).astype(jnp.bfloat16)
-    piece = lax.all_gather(normed, "tp", axis=0, tiled=True)
+    ring = [normed]
+    for hop in range(3):
+        ring.append(lax.ppermute(ring[-1], "tp", [(dev, (dev + 1) % 4) for dev in range(4)]))
+    piece = jnp.roll(
+        jnp.concatenate(ring[::-1], axis=0), (lax.axis_index("tp") + 1) * ring[0].shape[0], axis=0
+    )
     gate = jnp.dot(piece, gate_whole, preferred_element_type=jnp.float32)
     upward = jnp.dot(piece, up_whole, preferred_element_type=jnp.float32)
     hidden = (jax.nn.silu(gate) * upward).astype(jnp.bfloat16)

time: 421 us -> 397 us (0.943)
  waiting for transfers between devices: 330 us -> 292 us
  local copies, waits for them, and re-layouts: 17.4 us -> 29.1 us
    all_gather x1, waiting for transfers between devices: 39.1 us -> 0.01 us  [collect_weights(): lax.all_gather(gate_weight, 'sp', axis=0, tiled=True)]
    ppermute x0 -> x3, waiting for transfers between devices: none -> 30.4 us  [local(): lax.ppermute(ring[-1], 'tp', [(dev, (dev + 1) % 4) for dev in range(4)])]
    all_gather x1 -> x0, waiting for transfers between devices: 25 us -> none  [local(): piece = lax.all_gather(normed, 'tp', axis=0, tiled=True)]
    unnamed x17 -> x23, local copies, waits for them, and re-layouts: 4.74 us -> 16.4 us
    all_gather x1, waiting for transfers between devices: 92.5 us -> 81.7 us  [collect_weights(): lax.all_gather(up_weight, 'sp', axis=0, tiled=True)]
    all_gather x1, waiting for transfers between devices: 85.4 us -> 93 us  [collect_weights(): lax.all_gather(down_weight, 'sp', axis=1, tiled=True)]
  transfers between devices with their start and end apart: 8 -> 10, of which waited for: 6 -> 7; matrix products, arithmetic and copies ran while one was open for 5% -> 8% of each run, Pallas kernels for 0% -> 0%
where the time goes in v1:
time: 397 us; the launch traced here: 396 us
  waiting for transfers between devices  292 us (74%)
  matrix products  37.4 us (9%)
  local copies, waits for them, and re-layouts  29.1 us (7%)
  other arithmetic  15.2 us (4%)
  between operations  15.2 us (4%)
  starting transfers between devices  7.18 us (2%)
    all_gather x1, waiting for transfers between devices, collect_weights(): lax.all_gather(down_weight, 'sp', axis=1, tiled=True)  93 us
    all_gather x1, waiting for transfers between devices, collect_weights(): lax.all_gather(up_weight, 'sp', axis=0, tiled=True)  81.7 us
    reduce_scatter x1, waiting for transfers between devices, local(): lax.psum_scatter(jnp.dot(rows, out_weight, preferred_element_type=jnp.flo...  52.1 us
    reduce_scatter x1, waiting for transfers between devices, local(): lax.psum_scatter(jnp.dot(rows, down_whole, preferred_element_type=jnp.flo...  32.8 us
    ppermute x3, waiting for transfers between devices, local(): lax.ppermute(ring[-1], 'tp', [(dev, (dev + 1) % 4) for dev in range(4)])  30.4 us
    unnamed x23, local copies, waits for them, and re-layouts  16.4 us
    dot_general x1, matrix products, local(): jnp.dot(rows, down_whole, preferred_element_type=jnp.float32)  16.3 us
    dot_general x1, matrix products, local(): gate = jnp.dot(piece, gate_whole, preferred_element_type=jnp.float32)  9.5 us
  transfers between devices with their start and end apart: 10, of which 7 were waited for; matrix products, arithmetic and copies ran while one was open for 8% of the time, Pallas kernels for 0%

profile of v1, /device:TPU:0, one launch (start us, length us, event | category | flops | bytes accessed | tf_op | source)
XLA Modules:
  0.0 395.7 jit_solution(17871419639877126608)
XLA Ops:
  7.4 1.2 copy.24
  8.6 1.1 copy.25
  9.7 0.4 multiply_cosine_fusion
  10.2 0.7 fusion.24
  10.9 5.5 %collective-permute-start = (bf16[128,256]{0,1:T(8,128)(2,1)}, bf16[128,256]{0,1:T(8,128)(2,1)}, u32[]{:S(2)}, u32[]{:S(2)}) collective-permute-start(bf16[128,256]{0,1:T(8,128)(2,1)} %get-tuple-element.16), channel_id=1, source_target_pairs={{0,4},{4,8},{8,12},{12,16},{16,20},{20,24},{24,28},{1,5},{5,9},{9,... | collective-permute-start | bytes 196616 | tf_op jit(solution)/shard_map/ppermute | solution.py:18
  16.4 1.3 collective-permute-start.1
  17.9 1.4 copy.31
  19.5 1.2 fusion.16
  20.7 0.9 pad_maximum_fusion.1
  21.6 1.8 convert_element_type.55
  23.4 1.3 max.17
  24.8 2.1 pad_maximum_fusion.5
  26.8 1.9 copy.26
  28.7 1.9 copy.27
  30.6 1.9 copy.28
  32.5 1.2 pad_maximum_fusion
  33.7 1.2 fusion.34
  34.9 2.0 copy.30
  36.9 2.3 fusion.1
  39.3 2.9 copy-done.1
  42.3 1.9 fusion
  44.3 0.3 copy.29
  44.5 5.4 %fusion.14 = bf16[5,128,2,4,64]{1,4,3,2,0:T(8,128)(2,1)S(1)} fusion(bf16[5,384,2,64,1]{1,3,4,2,0:T(8,128)(2,1)S(1)} %bitcast.57, f32[5,2,384,128,4]{3,2,4,1,0:T(8,128)} %copy-done.1, f32[5,2,4,128]{3,2,1,0:T(4,128)S(1)} %exponential_add_fusion, f32[5,2,4,128]{3,2,1,0:T(4,128)S(1)} %broadcast_maximum_fusion, pred[5,128,384]{1,2,0:T(8,128)(4,1)S(1)} %fusion.16), kind=kOutput, calls=%fused_computation.21 | convolution fusion | flops 261816320 | bytes 9297920 | tf_op jit(solution)/shard_map/nkgqs,nskd->nqkgd/dot_general | solution.py:85
  50.0 0.5 copy.34
  50.5 3.9 fusion.19
  54.4 0.5 all-gather.4.cloned.1.call-update
  55.0 0.5 all-gather.6.cloned.1.call-update
  55.6 0.5 all-gather.8.cloned.1.call-update
  56.2 52.1 %reduce-scatter.3.cloned.1.call-done = f32[160,2048]{1,0:T(8,128)} async-done(((f32[640,2048]{1,0:T(8,128)}), f32[160,2048]{1,0:T(8,128)}) %reduce-scatter.3.cloned.1.call-update) | async-done | bytes 1310736 | tf_op jit(solution)/shard_map/reduce_scatter | solution.py:106
  108.3 1.6 fusion.10
  110.1 0.2 collective-permute-start.2
  110.4 10.0 %collective-permute-done.2 = bf16[160,2048]{1,0:T(8,128)(2,1)S(1)} collective-permute-done((bf16[160,2048]{1,0:T(8,128)(2,1)S(1)}, bf16[160,2048]{1,0:T(8,128)(2,1)S(1)}, u32[]{:S(2)}, u32[]{:S(2)}) %collective-permute-start.2) | collective-permute-done | bytes 655392 | tf_op jit(solution)/shard_map/ppermute | solution.py:118
  120.4 10.1 %collective-permute-done.3 = bf16[160,2048]{1,0:T(8,128)(2,1)} collective-permute-done((bf16[160,2048]{1,0:T(8,128)(2,1)S(1)}, bf16[160,2048]{1,0:T(8,128)(2,1)}, u32[]{:S(2)}, u32[]{:S(2)}) %collective-permute-start.3) | collective-permute-done | bytes 655392 | tf_op jit(solution)/shard_map/ppermute | solution.py:118
  130.5 10.3 %collective-permute-done.4 = bf16[160,2048]{1,0:T(8,128)(2,1)} collective-permute-done((bf16[160,2048]{1,0:T(8,128)(2,1)}, bf16[160,2048]{1,0:T(8,128)(2,1)}, u32[]{:S(2)}, u32[]{:S(2)}) %collective-permute-start.4) | collective-permute-done | bytes 655392 | tf_op jit(solution)/shard_map/ppermute | solution.py:118
  140.8 2.0 constant_dynamic-update-slice_fusion.7
  142.8 2.0 constant_dynamic-update-slice_fusion.6
  144.8 0.9 constant_dynamic-update-slice_fusion.5
  145.7 1.1 constant_dynamic-update-slice_fusion.4
  146.8 2.0 constant_dynamic-update-slice_fusion.3
  148.8 2.0 constant_dynamic-update-slice_fusion.2
  150.8 0.9 constant_dynamic-update-slice_fusion.1
  151.7 1.1 constant_dynamic-update-slice_fusion
  152.8 9.5 %fusion.5 = f32[640,1408]{1,0:T(8,128)} fusion(bf16[2048,1408]{1,0:T(8,128)(2,1)} %all-gather.4.cloned.1.call-done, bf16[1280,2048]{1,0:T(8,128)(2,1)} %constant_dynamic-update-slice_fusion, s32[]{:T(128)S(6)} %select_n.19), kind=kOutput, calls=%fused_computation.10 | convolution fusion | flops 3690987520 | bytes 11993092 | tf_op jit(solution)/shard_map/dot_general | solution.py:122
  162.3 81.7 %all-gather.6.cloned.1.call-done = bf16[2048,1408]{1,0:T(8,128)(2,1)} async-done(((bf16[256,1408]{1,0:T(8,128)(2,1)}), bf16[2048,1408]{1,0:T(8,128)(2,1)}) %all-gather.6.cloned.1.call-update) | async-done | bytes 5767184 | tf_op jit(solution)/shard_map/all_gather | solution.py:94
  244.0 93.0 %all-gather.8.cloned.1.call-done = bf16[1408,2048]{1,0:T(8,128)(2,1)} async-done(((bf16[1408,256]{1,0:T(8,128)(2,1)}), bf16[1408,2048]{1,0:T(8,128)(2,1)}) %all-gather.8.cloned.1.call-update) | async-done | bytes 5767184 | tf_op jit(solution)/shard_map/all_gather | solution.py:95
  336.9 16.3 %convolution_convert_fusion = bf16[640,2048]{1,0:T(8,128)(2,1)} fusion(bf16[1408,2048]{1,0:T(8,128)(2,1)} %all-gather.8.cloned.1.call-done, f32[640,1408]{1,0:T(8,128)} %fusion.5, bf16[2048,1408]{1,0:T(8,128)(2,1)} %all-gather.6.cloned.1.call-done, bf16[1280,2048]{1,0:T(8,128)(2,1)} %constant_dynamic-update-slice_fusion, s32[]{:T(128)S(6)} %select_n.19), kind=kOutput, calls=%fused_computation.7 | convolution fusion | flops 7388692480 | bytes 20381700 | tf_op jit(solution)/shard_map/dot_general | solution.py:127
  353.3 32.8 %reduce-scatter.5.cloned.1.call-done = bf16[160,2048]{1,0:T(8,128)(2,1)} async-done(((bf16[640,2048]{1,0:T(8,128)(2,1)}), bf16[160,2048]{1,0:T(8,128)(2,1)}) %reduce-scatter.5.cloned.1.call-update) | async-done | bytes 655376 | tf_op jit(solution)/shard_map/reduce_scatter | solution.py:126
  386.0 2.1 fusion.13
  (40 shorter events, 1.2 us)
Async XLA Ops:
  7.4 43.1 %copy-start = (bf16[512,2048]{1,0:T(8,128)(2,1)S(1)}, bf16[512,2048]{1,0:T(8,128)(2,1)}, u32[]{:S(2)}) copy-start(bf16[512,2048]{1,0:T(8,128)(2,1)} %param.15) | copy-start | bytes 6291460
  7.4 100.9 %reduce-scatter.3.cloned.1.call-start = ((), (), s32[]{:S(2)}) async-start(), calls=%async_computation.2 | async-start | bytes 6553600 | tf_op jit(solution)/shard_map/reduce_scatter | solution.py:106
  10.2 7.6 %copy-start.3 = (bf16[640,2,64]{0,2,1:T(8,128)(2,1)}, bf16[640,2,64]{0,2,1:T(8,128)(2,1)S(1)}, u32[]{:S(2)}) copy-start(bf16[640,2,64]{0,2,1:T(8,128)(2,1)S(1)} %pad_maximum_fusion.7) | copy-start | bytes 491524
  10.9 13.9 %collective-permute-start = (bf16[128,256]{0,1:T(8,128)(2,1)}, bf16[128,256]{0,1:T(8,128)(2,1)}, u32[]{:S(2)}, u32[]{:S(2)}) collective-permute-start(bf16[128,256]{0,1:T(8,128)(2,1)} %get-tuple-element.16), channel_id=1, source_target_pairs={{0,4},{4,8},{8,12},{12,16},{16,20},{20,24},{24,28},{1,5},{5,9},{9,... | collective-permute-start | bytes 196616 | tf_op jit(solution)/shard_map/ppermute | solution.py:18
  16.4 8.4 %collective-permute-start.1 = (bf16[128,256]{0,1:T(8,128)(2,1)}, bf16[128,256]{0,1:T(8,128)(2,1)}, u32[]{:S(2)}, u32[]{:S(2)}) collective-permute-start(bf16[128,256]{0,1:T(8,128)(2,1)} %get-tuple-element.17), channel_id=1, source_target_pairs={{4,0},{8,4},{12,8},{16,12},{20,16},{24,20},{28,24},{5,1},{9,5},{13... | collective-permute-start | bytes 196616 | tf_op jit(solution)/shard_map/ppermute | solution.py:20
  36.9 2.3 copy-start.6
  39.2 3.1 copy-start.1
  39.2 5.0 %copy-start.2 = (bf16[5,384,128]{2,1,0:T(8,128)(2,1)S(1)}, bf16[5,384,128]{2,1,0:T(8,128)(2,1)}, u32[]{:S(2)}) copy-start(bf16[5,384,128]{2,1,0:T(8,128)(2,1)} %get-tuple-element.10) | copy-start | bytes 1474564
  54.4 54.0 %copy-start.4 = (bf16[160,2048]{1,0:T(8,128)(2,1)S(1)}, bf16[160,2048]{1,0:T(8,128)(2,1)}, u32[]{:S(2)}) copy-start(bf16[160,2048]{1,0:T(8,128)(2,1)} %param.14) | copy-start | bytes 1966084
  54.4 55.6 %copy-start.5 = (f32[2048]{0:T(1024)S(1)}, f32[2048]{0:T(1024)}, u32[]{:S(2)}) copy-start(f32[2048]{0:T(1024)} %param.16) | copy-start | bytes 24580
  54.4 98.4 %all-gather.4.cloned.1.call-start = ((), (), s32[]{:S(2)}) async-start(), calls=%async_computation.3 | async-start | bytes 6488064 | tf_op jit(solution)/shard_map/all_gather | solution.py:93
  55.0 189.0 %all-gather.6.cloned.1.call-start = ((), (), s32[]{:S(2)}) async-start(), calls=%async_computation.4 | async-start | bytes 6488064 | tf_op jit(solution)/shard_map/all_gather | solution.py:94
  55.6 281.4 %all-gather.8.cloned.1.call-start = ((), (), s32[]{:S(2)}) async-start(), calls=%async_computation.5 | async-start | bytes 6488064 | tf_op jit(solution)/shard_map/all_gather | solution.py:95
  56.1 329.9 %reduce-scatter.5.cloned.1.call-start = ((), (), s32[]{:S(2)}) async-start(), calls=%async_computation.6 | async-start | bytes 3276800 | tf_op jit(solution)/shard_map/reduce_scatter | solution.py:126
  110.1 10.2 %collective-permute-start.2 = (bf16[160,2048]{1,0:T(8,128)(2,1)S(1)}, bf16[160,2048]{1,0:T(8,128)(2,1)S(1)}, u32[]{:S(2)}, u32[]{:S(2)}) collective-permute-start(bf16[160,2048]{1,0:T(8,128)(2,1)S(1)} %fusion.12), channel_id=1, source_target_pairs={{0,1},{1,2},{2,3},{3,0},{4,5},{5,6},{6,7},{7,4},{8,9},{9,10},{10,1... | collective-permute-start | bytes 1966088 | tf_op jit(solution)/shard_map/ppermute | solution.py:118
  120.4 10.1 %collective-permute-start.3 = (bf16[160,2048]{1,0:T(8,128)(2,1)S(1)}, bf16[160,2048]{1,0:T(8,128)(2,1)}, u32[]{:S(2)}, u32[]{:S(2)}) collective-permute-start(bf16[160,2048]{1,0:T(8,128)(2,1)S(1)} %collective-permute-done.2), channel_id=1, source_target_pairs={{0,1},{1,2},{2,3},{3,0},{4,5},{5,6},{6,7},{7,4},{8,9},{9,10},{10,1... | collective-permute-start | bytes 1966088 | tf_op jit(solution)/shard_map/ppermute | solution.py:118
  130.5 10.3 %collective-permute-start.4 = (bf16[160,2048]{1,0:T(8,128)(2,1)}, bf16[160,2048]{1,0:T(8,128)(2,1)}, u32[]{:S(2)}, u32[]{:S(2)}) collective-permute-start(bf16[160,2048]{1,0:T(8,128)(2,1)} %collective-permute-done.3), channel_id=1, source_target_pairs={{0,1},{1,2},{2,3},{3,0},{4,5},{5,6},{6,7},{7,4},{8,9},{9,10},{10,1... | collective-permute-start | bytes 1966088 | tf_op jit(solution)/shard_map/ppermute | solution.py:118
Sparse Core Ops, SparseCore 0:
  54.5 53.7 reduce-scatter.2
  353.4 32.6 reduce-scatter.4
Sparse Core Ops, SparseCore 1:
  57.1 94.5 all-gather.3
  153.7 90.2 all-gather.5
  245.9 91.0 all-gather.7
